TPU v7x, 512 devices: a whole 4x4x16 slice. The times are simulated.
512 devices in a mesh: fs: 64 (over z, y), tp: 8 (over x, core).
Axes of the slice: x: 4, y: 4, z: 16, core: 2. Of those that a mesh axis runs over, the one named last changes fastest.
Arguments:
- tokens: bfloat16 [49152, 2048], P('fs'), may hold values from -6 to 6
- norm_gain: float32 [2048], replicated, may hold values from 0.1 to 1.9
- gate_weight: float32 [2048, 5120], P('fs', 'tp'), may hold values from -0.125 to 0.125
- value_weight: float32 [2048, 5120], P('fs', 'tp'), may hold values from -0.125 to 0.125
- gate_scale: float32 [5120], P('tp'), may hold values from 0.3 to 3
- value_scale: float32 [5120], P('tp'), may hold values from 0.3 to 3
- gate_kernel: float32 [3, 5120], P(None, 'tp'), may hold values from -3.5 to 3.5
- value_kernel: float32 [3, 5120], P(None, 'tp'), may hold values from -3.5 to 3.5
- gate_bias: float32 [5120], P('tp'), may hold values from -3 to 3
- value_bias: float32 [5120], P('tp'), may hold values from -3 to 3
- down_weight: float32 [5120, 2048], P('tp', 'fs'), may hold values from -0.078125 to 0.078125
- down_scale: float32 [2048], P('tp'), may hold values from 0.3 to 3
Outputs:
- mixed: bfloat16 [49152, 2048], P('fs', 'tp')
All inputs are finite; a program needn't handle non-finite values.
Results may differ from a plain program's by a relative error of at most 0.014.
Values may be sent and summed in bfloat16 or wider, within the bound.
No kernel may reach another device: no remote copies, remote signals or barrier semaphores. Data moves between devices by JAX's collectives and lax.ppermute only.
A program may use at most 64 MiB of HBM per device.

v0:
```python
import jax
import jax.numpy as jnp
from jax import lax
from jax.experimental.layout import Layout, with_layout_constraint
from jax.sharding import Mesh, PartitionSpec as P

epsilon = 1e-06
up_lift = 2.0**17
down_lift = 2.0**19


def down_half(hidden, rows, core):
    groups, _, part, total = rows.shape
    units = hidden.shape[1]
    mine = lax.dynamic_slice(rows, (0, core, 0, total - units), (groups, 1, part, units))
    mine = mine.reshape(groups * part, units).astype(jnp.bfloat16)
    product = lax.dot_general(
        mine, hidden, (((1,), (1,)), ((), ())), preferred_element_type=jnp.float32
    )
    return product.reshape(groups, part, -1)


def causal_mix(current, previous, kernel, tap_bias):
    row_count = current.shape[0]
    joined = jnp.concatenate([previous, current], axis=0).astype(jnp.float32)
    summed_taps = tap_bias[None, :] + kernel[2][None, :] * joined[2:]
    for back_by in (1, 2):
        summed_taps = (
            summed_taps
            + kernel[2 - back_by][None, :] * joined[2 - back_by : 2 - back_by + row_count]
        )
    return summed_taps


def body(
    tokens,
    norm_gain,
    gate_weight,
    value_weight,
    gate_scale,
    value_scale,
    gate_kernel,
    value_kernel,
    gate_bias,
    value_bias,
    down_weight,
    down_scale,
):
    z_count, y_count = (lax.axis_size("z"), lax.axis_size("y"))
    x_count, c_count = (lax.axis_size("x"), lax.axis_size("c"))
    place = lax.axis_index("z") * y_count + lax.axis_index("y")
    core = lax.axis_index("c")
    row_count, width = tokens.shape
    piece, units = gate_weight.shape
    gain = lax.dynamic_slice(norm_gain, (place * piece,), (piece,))[:, None] * up_lift
    shard = jnp.concatenate(
        [gate_weight * gain, value_weight * gain, down_weight.T * down_lift], axis=1
    ).astype(jnp.float16)
    over_z = lax.all_gather(shard, "z", axis=0)
    full = lax.all_gather(over_z, "y", axis=1, tiled=True).reshape(width, 3 * units)
    tokens, full = lax.optimization_barrier((tokens, full))
    values = tokens.astype(jnp.float32)
    factor = lax.rsqrt(jnp.mean(values * values, axis=1, keepdims=True) + epsilon) / up_lift
    pre = []
    for at, scale in ((0, gate_scale), (units, value_scale)):
        raw = jnp.dot(
            tokens,
            full[:, at : at + units].astype(jnp.bfloat16),
            preferred_element_type=jnp.float32,
        )
        pre.append((raw * (factor * scale[None, :])).astype(jnp.bfloat16))
    tails = jnp.concatenate([p[row_count - 2 :] for p in pre], axis=1)
    previous = lax.ppermute(
        tails, ("z", "y"), [(source, source + 1) for source in range(z_count * y_count - 1)]
    )
    gate_conv = causal_mix(pre[0], previous[:, :units], gate_kernel, gate_bias)
    value_conv = causal_mix(pre[1], previous[:, units:], value_kernel, value_bias)
    hidden = (jax.nn.gelu(gate_conv, approximate=True) * value_conv).astype(jnp.bfloat16)
    hidden = with_layout_constraint(hidden, Layout(major_to_minor=(0, 1)))
    rows = full.reshape(x_count, c_count, width // (x_count * c_count), 3 * units)
    sent = down_half(hidden, rows, 1 - core).astype(jnp.bfloat16)
    received = lax.ppermute(sent, "c", [(0, 1), (1, 0)])
    kept = lax.optimization_barrier(down_half(hidden, rows, core))
    paired = (kept + received.astype(jnp.float32)).astype(jnp.bfloat16)
    last_scale, paired = lax.optimization_barrier((down_scale / down_lift, paired))
    parts = lax.all_to_all(paired, "x", 0, 0)
    summed = jnp.sum(parts.astype(jnp.float32), axis=0) * last_scale[:, None]
    return summed.astype(jnp.bfloat16).T


def solution(mesh):
    grid = Mesh(mesh.devices.reshape(16, 4, 4, 2), ("z", "y", "x", "c"))
    fs, tp = (("z", "y"), ("x", "c"))
    return jax.shard_map(
        body,
        mesh=grid,
        in_specs=(
            P(fs, None),
            P(),
            P(fs, tp),
            P(fs, tp),
            P(tp),
            P(tp),
            P(None, tp),
            P(None, tp),
            P(tp),
            P(tp),
            P(tp, fs),
            P(tp),
        ),
        out_specs=P(fs, tp),
        check_vma=False,
    )
```

profile of v0, /device:TPU:32, one launch (start us, length us, event | category | flops | bytes accessed | tf_op | source)
XLA Modules:
  0.0 164.0 jit_solution(14825666330794606886)
XLA Ops:
  0.0 0.9 fusion.37
  0.9 0.8 dynamic-slice_multiply_fusion
  1.7 1.0 fusion.35
  2.7 46.4 %all-gather.2 = f16[16,32,1920]{2,1,0:T(8,128)(2,1)S(1)} all-gather(f16[1,32,1920]{2,1,0:T(8,128)(2,1)S(1)} %pad_maximum_fusion), channel_id=1, replica_groups=mesh['z'=16,'y'=4,'x'=4,'c'=2] {'z'}, dimensions={0}, use_global_device_ids=true | all-gather | bytes 2088960 | tf_op jit(solution)/shard_map/all_gather | solution.py:59
  49.2 61.7 %all-gather.3 = f16[16,128,1920]{2,1,0:T(8,128)(2,1)S(1)} all-gather(f16[16,32,1920]{2,1,0:T(8,128)(2,1)S(1)} %all-gather.2), channel_id=1, replica_groups=mesh['z'=16,'y'=4,'x'=4,'c'=2] {'y'}, dimensions={1}, use_global_device_ids=true | all-gather | bytes 9830400 | tf_op jit(solution)/shard_map/all_gather | solution.py:60
  110.9 0.0 copy-done.1
  110.9 0.7 multiply_reduce_fusion
  111.6 0.0 copy-done.7
  111.6 0.0 copy-start.8
  111.6 2.6 %multiply_convert_fusion = bf16[768,640]{1,0:T(8,128)(2,1)S(1)} fusion(bf16[768,2048]{1,0:T(8,128)(2,1)S(1)} %copy-done.1, f16[2048,1920]{1,0:T(8,128)(2,1)S(1)} %bitcast.35, f32[640]{0:T(1024)S(1)} %copy-done.7, f32[768]{0:T(1024)S(1)} %rsqrt_multiply_fusion), kind=kOutput, calls=%fused_computation.31 | convolution fusion | flops 2016051200 | bytes 6758400 | tf_op jit(solution)/shard_map/dot_general | solution.py:66
  114.2 0.0 copy-done
  114.2 0.0 copy-done.8
  114.2 0.0 copy-start.2
  114.3 0.0 copy-start.3
  114.3 2.6 %multiply_convert_fusion.1 = bf16[768,640]{1,0:T(8,128)(2,1)S(1)} fusion(bf16[768,2048]{1,0:T(8,128)(2,1)S(1)} %copy-done.1, f16[2048,1920]{1,0:T(8,128)(2,1)S(1)} %bitcast.36, f32[640]{0:T(1024)S(1)} %copy-done.8, f32[768]{0:T(1024)S(1)} %rsqrt_multiply_fusion), kind=kOutput, calls=%fused_computation.32 | convolution fusion | flops 2016051200 | bytes 6758400 | tf_op jit(solution)/shard_map/dot_general | solution.py:66
  116.9 3.2 %collective-permute-start = (bf16[2,1280]{1,0:T(2,128)(2,1)S(1)}, bf16[2,1280]{1,0:T(2,128)(2,1)S(1)}, u32[]{:S(2)}, u32[]{:S(2)}) collective-permute-start(bf16[2,1280]{1,0:T(2,128)(2,1)S(1)} %pad_maximum_fusion.1), channel_id=1, source_target_pairs={{0,8},{8,16},{16,24},{24,32},{32,40},{40,48},{48,56},{56,64},{64,7... | collective-permute-start | bytes 15368 | tf_op jit(solution)/shard_map/ppermute | solution.py:73
  120.2 4.8 %collective-permute-done = bf16[2,1280]{1,0:T(2,128)(2,1)S(1)} collective-permute-done((bf16[2,1280]{1,0:T(2,128)(2,1)S(1)}, bf16[2,1280]{1,0:T(2,128)(2,1)S(1)}, u32[]{:S(2)}, u32[]{:S(2)}) %collective-permute-start) | collective-permute-done | bytes 5152 | tf_op jit(solution)/shard_map/ppermute | solution.py:73
  125.0 0.0 copy-start.5
  125.0 0.4 maximum_convert_fusion
  125.4 0.3 copy-done.4
  125.7 0.0 copy-done.5
  125.7 2.0 %fusion.14 = bf16[768,640]{1,0:T(8,128)(2,1)S(1)} fusion(f32[770,640]{1,0:T(8,128)S(1)} %get-tuple-element.24, f32[770,640]{1,0:T(8,128)S(1)} %get-tuple-element.23, f32[640]{0:T(1024)S(1)} %get-tuple-element.17, f32[640]{0:T(1024)S(1)} %get-tuple-element.18, f32[640]{0:T(1024)S(1)} %get-tuple-element.16, f32[640]{0:T(1024)S(1)} %copy-done.4, ...), kind=kLoop, calls=%fused_computation.18 | loop fusion | flops 10813440 | bytes 12800000 | tf_op jit(solution)/shard_map/convert_element_type | solution.py:78
  127.7 0.0 copy-start.6
  127.7 4.0 %convolution_convert_fusion = bf16[4,256,768]{2,1,0:T(8,128)(2,1)} fusion(f16[4,2,256,1920]{3,2,1,0:T(8,128)(2,1)} %bitcast.37, s32[]{:T(128)S(6)} %select_n.11, bf16[768,640]{1,0:T(8,128)(2,1)S(1)} %fusion.14), kind=kOutput, calls=%fused_computation.33 | convolution fusion | flops 1008074752 | bytes 3866628 | tf_op jit(solution)/shard_map/dot_general | solution.py:17
  131.7 1.9 %collective-permute-start.1 = (bf16[4,256,768]{2,1,0:T(8,128)(2,1)}, bf16[4,256,768]{2,1,0:T(8,128)(2,1)S(1)}, u32[]{:S(2)}, u32[]{:S(2)}) collective-permute-start(bf16[4,256,768]{2,1,0:T(8,128)(2,1)} %convolution_convert_fusion), channel_id=1, source_target_pairs={{0,1},{1,0},{2,3},{3,2},{4,5},{5,4},{6,7},{7,6},{8,9},{9,8},{10,11... | collective-permute-start | bytes 4718600 | tf_op jit(solution)/shard_map/ppermute | solution.py:82
  133.6 2.8 %fusion.28 = f32[4,256,768]{2,1,0:T(8,128)S(1)} fusion(f16[4,2,256,1920]{3,2,1,0:T(8,128)(2,1)} %bitcast.38, s32[]{:T(128)S(6)} %select_n.10, bf16[768,640]{1,0:T(8,128)(2,1)S(1)} %fusion.14), kind=kOutput, calls=%fused_computation.38 | convolution fusion | flops 1007288320 | bytes 5439492 | tf_op jit(solution)/shard_map/dot_general | solution.py:17
  136.4 0.8 collective-permute-done.1
  137.2 0.4 add_convert_fusion
  137.7 25.1 %all_to_all.5 = bf16[4,256,768]{2,1,0:T(8,128)(2,1)S(1)} all-to-all(bf16[4,256,768]{2,1,0:T(8,128)(2,1)S(1)} %add_convert_fusion), channel_id=1, replica_groups=mesh['z'=16,'y'=4,'x'=4,'c'=2] {'x'}, dimensions={0} | all-to-all | bytes 3145728 | tf_op jit(solution)/shard_map/all_to_all | solution.py:86
  162.8 0.2 convert_reduce_fusion
  163.0 0.1 fusion.34
  163.1 0.9 copy.17
  (15 shorter events, 0.1 us)
Async XLA Ops:
  49.2 61.7 %copy-start.1 = (bf16[768,2048]{1,0:T(8,128)(2,1)S(1)}, bf16[768,2048]{1,0:T(8,128)(2,1)}, u32[]{:S(2)}) copy-start(bf16[768,2048]{1,0:T(8,128)(2,1)} %param.12) | copy-start | bytes 9437188
  110.9 3.4 %copy-start = (f16[16,128,1920]{2,1,0:T(8,128)(2,1)}, f16[16,128,1920]{2,1,0:T(8,128)(2,1)S(1)}, u32[]{:S(2)}) copy-start(f16[16,128,1920]{2,1,0:T(8,128)(2,1)S(1)} %all-gather.3) | copy-start | bytes 23592964
  110.9 0.7 copy-start.7
  111.6 2.7 %copy-start.8 = (f32[640]{0:T(1024)S(1)}, f32[640]{0:T(1024)}, u32[]{:S(2)}) copy-start(f32[640]{0:T(1024)} %param.16) | copy-start | bytes 7684
  114.2 5.9 %copy-start.2 = (f32[3,640]{1,0:T(4,128)S(1)}, f32[3,640]{1,0:T(4,128)}, u32[]{:S(2)}) copy-start(f32[3,640]{1,0:T(4,128)} %param.19) | copy-start | bytes 23044
  114.3 5.9 %copy-start.3 = (f32[3,640]{1,0:T(4,128)S(1)}, f32[3,640]{1,0:T(4,128)}, u32[]{:S(2)}) copy-start(f32[3,640]{1,0:T(4,128)} %param.18) | copy-start | bytes 23044
  116.9 8.0 %collective-permute-start = (bf16[2,1280]{1,0:T(2,128)(2,1)S(1)}, bf16[2,1280]{1,0:T(2,128)(2,1)S(1)}, u32[]{:S(2)}, u32[]{:S(2)}) collective-permute-start(bf16[2,1280]{1,0:T(2,128)(2,1)S(1)} %pad_maximum_fusion.1), channel_id=1, source_target_pairs={{0,8},{8,16},{16,24},{24,32},{32,40},{40,48},{48,56},{56,64},{64,7... | collective-permute-start | bytes 15368 | tf_op jit(solution)/shard_map/ppermute | solution.py:73
  125.0 0.7 copy-start.4
  125.0 0.7 copy-start.5
  127.7 5.9 %copy-start.6 = (f32[256]{0:T(256)S(1)}, f32[256]{0:T(256)}, u32[]{:S(2)}) copy-start(f32[256]{0:T(256)} %param.23) | copy-start | bytes 3076
  131.7 5.5 %collective-permute-start.1 = (bf16[4,256,768]{2,1,0:T(8,128)(2,1)}, bf16[4,256,768]{2,1,0:T(8,128)(2,1)S(1)}, u32[]{:S(2)}, u32[]{:S(2)}) collective-permute-start(bf16[4,256,768]{2,1,0:T(8,128)(2,1)} %convolution_convert_fusion), channel_id=1, source_target_pairs={{0,1},{1,0},{2,3},{3,2},{4,5},{5,4},{6,7},{7,6},{8,9},{9,8},{10,11... | collective-permute-start | bytes 4718600 | tf_op jit(solution)/shard_map/ppermute | solution.py:82
where the time goes:
time: 164 us
  blocking collectives  133 us (81%)
  matrix products  12 us (7%)
  other arithmetic  6.59 us (4%)
  waiting for transfers between devices  5.54 us (3%)
  starting transfers between devices  5.1 us (3%)
    all_gather x1, blocking collectives, body(): lax.all_gather(over_z, 'y', axis=1, tiled=True).reshape(width, 3 * units)  61.7 us
    all_gather x1, blocking collectives, body(): over_z = lax.all_gather(shard, 'z', axis=0)  46.4 us
    all_to_all x1, blocking collectives, body(): parts = lax.all_to_all(paired, 'x', 0, 0)  25.1 us
    dot_general x2, matrix products, down_half(): lax.dot_general(mine, hidden, (((1,), (1,)), ((), ())), preferred_element...  6.78 us
    dot_general x2, matrix products, body(): jnp.dot(tokens, full[:, at:at + units].astype(jnp.bfloat16), preferred_el...  5.24 us
    ppermute x1, waiting for transfers between devices, body(): lax.ppermute(tails, ('z', 'y'), [(source, source + 1) for source in range...  4.76 us
  transfers between devices with their start and end apart: 2, of which 2 were waited for; matrix products, arithmetic and copies ran while one was open for 2% of the time, Pallas kernels for 0%

commit v1 on v0

--- a/solution.py
+++ b/solution.py
@@ -1,12 +1,29 @@
+import functools
 import jax
 import jax.numpy as jnp
 from jax import lax
 from jax.experimental.layout import Layout, with_layout_constraint
 from jax.sharding import Mesh, PartitionSpec as P
+from jax.lax import all_to_all, axis_size
 
 epsilon = 1e-06
 up_lift = 2.0**17
 down_lift = 2.0**19
+
+
+def treat_zones(unit, along_axis, pos_dim):
+    return jnp.concatenate(
+        all_to_all(
+            jnp.stack([unit for _ in range(axis_size(along_axis))], 0),
+            axis_name=along_axis,
+            split_axis=0,
+            concat_axis=0,
+        ),
+        pos_dim,
+    )
+
+
+unite_scales_all = functools.partial(treat_zones, along_axis="y", pos_dim=1)
 
 
 def down_half(hidden, rows, core):
@@ -57,7 +74,7 @@
         [gate_weight * gain, value_weight * gain, down_weight.T * down_lift], axis=1
     ).astype(jnp.float16)
     over_z = lax.all_gather(shard, "z", axis=0)
-    full = lax.all_gather(over_z, "y", axis=1, tiled=True).reshape(width, 3 * units)
+    full = unite_scales_all(over_z).reshape(width, 3 * units)
     tokens, full = lax.optimization_barrier((tokens, full))
     values = tokens.astype(jnp.float32)
     factor = lax.rsqrt(jnp.mean(values * values, axis=1, keepdims=True) + epsilon) / up_lift

time: 164 us -> 200 us (1.22)
  blocking collectives: 133 us -> 158 us
  local copies, waits for them, and re-layouts: 1.31 us -> 7.02 us
  matrix products: 12 us -> 15.5 us
  other arithmetic: 6.59 us -> 8.63 us
    all_to_all x0 -> x1, blocking collectives: none -> 86 us  [treat_zones(): all_to_all(jnp.stack([unit for _ in range(axis_size(along_axis))], 0), ax...]
    all_gather x1 -> x0, blocking collectives: 61.7 us -> none  [body(): lax.all_gather(over_z, 'y', axis=1, tiled=True).reshape(width, 3 * units)]
    all_to_all x0 -> x1, local copies, waits for them, and re-layouts: none -> 4.92 us  [treat_zones(): all_to_all(jnp.stack([unit for _ in range(axis_size(along_axis))], 0), ax...]
    dot_general x2, matrix products: 5.24 us -> 8.75 us  [body(): jnp.dot(tokens, full[:, at:at + units].astype(jnp.bfloat16), preferred_el...]
    reduce_sum x1, other arithmetic: 0.68 us -> 2.72 us  [body(): jnp.mean(values * values, axis=1, keepdims=True) + epsilon]
  transfers between devices with their start and end apart: 2 -> 2, of which waited for: 2 -> 2; matrix products, arithmetic and copies ran while one was open for 2% -> 1% of each run, Pallas kernels for 0% -> 0%
where the time goes in v1:
time: 200 us; the launch traced here: 199 us
  blocking collectives  158 us (79%)
  matrix products  15.5 us (8%)
  other arithmetic  8.63 us (4%)
  local copies, waits for them, and re-layouts  7.02 us (4%)
  waiting for transfers between devices  5.85 us (3%)
  starting transfers between devices  4.38 us (2%)
    all_to_all x1, blocking collectives, treat_zones(): all_to_all(jnp.stack([unit for _ in range(axis_size(along_axis))], 0), ax...  86 us
    all_gather x1, blocking collectives, body(): over_z = lax.all_gather(shard, 'z', axis=0)  46.4 us
    all_to_all x1, blocking collectives, body(): parts = lax.all_to_all(paired, 'x', 0, 0)  25.1 us
    dot_general x2, matrix products, body(): jnp.dot(tokens, full[:, at:at + units].astype(jnp.bfloat16), preferred_el...  8.75 us
    dot_general x2, matrix products, down_half(): lax.dot_general(mine, hidden, (((1,), (1,)), ((), ())), preferred_element...  6.78 us
    ppermute x1, waiting for transfers between devices, body(): lax.ppermute(tails, ('z', 'y'), [(source, source + 1) for source in range...  5.06 us
    all_to_all x1, local copies, waits for them, and re-layouts, treat_zones(): all_to_all(jnp.stack([unit for _ in range(axis_size(along_axis))], 0), ax...  4.92 us
  transfers between devices with their start and end apart: 2, of which 2 were waited for; matrix products, arithmetic and copies ran while one was open for 1% of the time, Pallas kernels for 0%

profile of v1, /device:TPU:32, one launch (start us, length us, event | category | flops | bytes accessed | tf_op | source)
XLA Modules:
  0.0 199.1 jit_solution(8666482871790693275)
XLA Ops:
  0.0 0.9 fusion.37
  0.9 0.8 dynamic-slice_multiply_fusion
  1.7 1.0 fusion.35
  2.7 46.4 %all-gather.1 = f16[16,32,1920]{2,1,0:T(8,128)(2,1)S(1)} all-gather(f16[1,32,1920]{2,1,0:T(8,128)(2,1)S(1)} %pad_maximum_fusion), channel_id=1, replica_groups=mesh['z'=16,'y'=4,'x'=4,'c'=2] {'z'}, dimensions={0}, use_global_device_ids=true | all-gather | bytes 2088960 | tf_op jit(solution)/shard_map/all_gather | solution.py:76
  49.2 0.7 stack.2
  49.9 86.0 %all_to_all.10 = f16[4,16,32,1920]{3,2,1,0:T(8,128)(2,1)S(1)} all-to-all(f16[4,16,32,1920]{3,2,1,0:T(8,128)(2,1)S(1)} %stack.2), channel_id=1, replica_groups=mesh['z'=16,'y'=4,'x'=4,'c'=2] {'y'}, dimensions={0} | all-to-all | bytes 15728640 | tf_op jit(solution)/shard_map/all_to_all | solution.py:16
  135.8 4.9 %copy.15 = f16[4,16,32,1920]{3,2,0,1:T(8,128)(2,1)} copy(f16[4,16,32,1920]{3,2,1,0:T(8,128)(2,1)S(1)} %all_to_all.10) | data formatting | bytes 15728640 | tf_op jit(solution)/shard_map/all_to_all | solution.py:16
  140.8 2.7 %multiply_reduce_fusion = f32[768]{0:T(1024)S(1)} fusion(bf16[768,2048]{1,0:T(8,128)(2,1)} %param.12), kind=kLoop, calls=%fused_computation | loop fusion | flops 4717824 | bytes 3148800 | tf_op jit(solution)/shard_map/reduce_sum | solution.py:80
  143.5 0.1 copy-done
  143.6 0.0 copy-done.6
  143.6 4.4 %multiply_convert_fusion = bf16[768,640]{1,0:T(8,128)(2,1)S(1)} fusion(bf16[768,2048]{1,0:T(8,128)(2,1)S(1)} %copy-done, f16[2048,1920]{1,0:T(8,128)(2,1)} %bitcast.37, f32[640]{0:T(1024)S(1)} %copy-done.6, f32[768]{0:T(1024)S(1)} %rsqrt_multiply_fusion), kind=kOutput, calls=%fused_computation.31 | convolution fusion | flops 2016051200 | bytes 6755840 | tf_op jit(solution)/shard_map/dot_general | solution.py:83
  148.0 0.0 copy-done.7
  148.0 0.0 copy-start.1
  148.0 0.0 copy-start.2
  148.0 4.4 %multiply_convert_fusion.1 = bf16[768,640]{1,0:T(8,128)(2,1)S(1)} fusion(bf16[768,2048]{1,0:T(8,128)(2,1)S(1)} %copy-done, f16[2048,1920]{1,0:T(8,128)(2,1)} %bitcast.38, f32[640]{0:T(1024)S(1)} %copy-done.7, f32[768]{0:T(1024)S(1)} %rsqrt_multiply_fusion), kind=kOutput, calls=%fused_computation.32 | convolution fusion | flops 2016051200 | bytes 6755840 | tf_op jit(solution)/shard_map/dot_general | solution.py:83
  152.4 2.5 %collective-permute-start = (bf16[2,1280]{1,0:T(2,128)(2,1)S(1)}, bf16[2,1280]{1,0:T(2,128)(2,1)S(1)}, u32[]{:S(2)}, u32[]{:S(2)}) collective-permute-start(bf16[2,1280]{1,0:T(2,128)(2,1)S(1)} %pad_maximum_fusion.1), channel_id=1, source_target_pairs={{0,8},{8,16},{16,24},{24,32},{32,40},{40,48},{48,56},{56,64},{64,7... | collective-permute-start | bytes 15368 | tf_op jit(solution)/shard_map/ppermute | solution.py:90
  155.0 5.1 %collective-permute-done = bf16[2,1280]{1,0:T(2,128)(2,1)S(1)} collective-permute-done((bf16[2,1280]{1,0:T(2,128)(2,1)S(1)}, bf16[2,1280]{1,0:T(2,128)(2,1)S(1)}, u32[]{:S(2)}, u32[]{:S(2)}) %collective-permute-start) | collective-permute-done | bytes 5152 | tf_op jit(solution)/shard_map/ppermute | solution.py:90
  160.1 0.0 copy-start.4
  160.1 0.4 maximum_convert_fusion
  160.5 0.3 copy-done.3
  160.7 0.0 copy-done.4
  160.8 2.0 %fusion.14 = bf16[768,640]{1,0:T(8,128)(2,1)S(1)} fusion(f32[770,640]{1,0:T(8,128)S(1)} %get-tuple-element.24, f32[770,640]{1,0:T(8,128)S(1)} %get-tuple-element.23, f32[640]{0:T(1024)S(1)} %get-tuple-element.17, f32[640]{0:T(1024)S(1)} %get-tuple-element.18, f32[640]{0:T(1024)S(1)} %get-tuple-element.16, f32[640]{0:T(1024)S(1)} %copy-done.3, ...), kind=kLoop, calls=%fused_computation.18 | loop fusion | flops 10813440 | bytes 12800000 | tf_op jit(solution)/shard_map/convert_element_type | solution.py:95
  162.8 0.0 copy-start.5
  162.8 4.0 %convolution_convert_fusion = bf16[4,256,768]{2,1,0:T(8,128)(2,1)} fusion(f16[4,2,256,1920]{3,2,1,0:T(8,128)(2,1)} %bitcast.39, s32[]{:T(128)S(6)} %select_n.11, bf16[768,640]{1,0:T(8,128)(2,1)S(1)} %fusion.14), kind=kOutput, calls=%fused_computation.33 | convolution fusion | flops 1008074752 | bytes 3866628 | tf_op jit(solution)/shard_map/dot_general | solution.py:34
  166.8 1.9 collective-permute-start.1
  168.7 2.8 %fusion.28 = f32[4,256,768]{2,1,0:T(8,128)S(1)} fusion(f16[4,2,256,1920]{3,2,1,0:T(8,128)(2,1)} %bitcast.40, s32[]{:T(128)S(6)} %select_n.10, bf16[768,640]{1,0:T(8,128)(2,1)S(1)} %fusion.14), kind=kOutput, calls=%fused_computation.38 | convolution fusion | flops 1007288320 | bytes 5439492 | tf_op jit(solution)/shard_map/dot_general | solution.py:34
  171.5 0.8 collective-permute-done.1
  172.3 0.4 add_convert_fusion
  172.7 25.1 %all_to_all.11 = bf16[4,256,768]{2,1,0:T(8,128)(2,1)S(1)} all-to-all(bf16[4,256,768]{2,1,0:T(8,128)(2,1)S(1)} %add_convert_fusion), channel_id=1, replica_groups=mesh['z'=16,'y'=4,'x'=4,'c'=2] {'x'}, dimensions={0} | all-to-all | bytes 3145728 | tf_op jit(solution)/shard_map/all_to_all | solution.py:103
  197.8 0.2 convert_reduce_fusion
  198.1 0.1 fusion.34
  198.2 0.9 copy.18
  (15 shorter events, 0.1 us)
Async XLA Ops:
  140.7 2.8 %copy-start = (bf16[768,2048]{1,0:T(8,128)(2,1)S(1)}, bf16[768,2048]{1,0:T(8,128)(2,1)}, u32[]{:S(2)}) copy-start(bf16[768,2048]{1,0:T(8,128)(2,1)} %param.12) | copy-start | bytes 9437188
  140.7 2.8 %copy-start.6 = (f32[640]{0:T(1024)S(1)}, f32[640]{0:T(1024)}, u32[]{:S(2)}) copy-start(f32[640]{0:T(1024)} %param.17) | copy-start | bytes 7684
  143.6 4.4 %copy-start.7 = (f32[640]{0:T(1024)S(1)}, f32[640]{0:T(1024)}, u32[]{:S(2)}) copy-start(f32[640]{0:T(1024)} %param.16) | copy-start | bytes 7684
  148.0 6.9 %copy-start.1 = (f32[3,640]{1,0:T(4,128)S(1)}, f32[3,640]{1,0:T(4,128)}, u32[]{:S(2)}) copy-start(f32[3,640]{1,0:T(4,128)} %param.19) | copy-start | bytes 23044
  148.0 6.9 %copy-start.2 = (f32[3,640]{1,0:T(4,128)S(1)}, f32[3,640]{1,0:T(4,128)}, u32[]{:S(2)}) copy-start(f32[3,640]{1,0:T(4,128)} %param.18) | copy-start | bytes 23044
  152.4 7.6 %collective-permute-start = (bf16[2,1280]{1,0:T(2,128)(2,1)S(1)}, bf16[2,1280]{1,0:T(2,128)(2,1)S(1)}, u32[]{:S(2)}, u32[]{:S(2)}) collective-permute-start(bf16[2,1280]{1,0:T(2,128)(2,1)S(1)} %pad_maximum_fusion.1), channel_id=1, source_target_pairs={{0,8},{8,16},{16,24},{24,32},{32,40},{40,48},{48,56},{56,64},{64,7... | collective-permute-start | bytes 15368 | tf_op jit(solution)/shard_map/ppermute | solution.py:90
  160.1 0.7 copy-start.3
  160.1 0.7 copy-start.4
  162.8 5.9 %copy-start.5 = (f32[256]{0:T(256)S(1)}, f32[256]{0:T(256)}, u32[]{:S(2)}) copy-start(f32[256]{0:T(256)} %param.23) | copy-start | bytes 3076
  166.8 5.5 %collective-permute-start.1 = (bf16[4,256,768]{2,1,0:T(8,128)(2,1)}, bf16[4,256,768]{2,1,0:T(8,128)(2,1)S(1)}, u32[]{:S(2)}, u32[]{:S(2)}) collective-permute-start(bf16[4,256,768]{2,1,0:T(8,128)(2,1)} %convolution_convert_fusion), channel_id=1, source_target_pairs={{0,1},{1,0},{2,3},{3,2},{4,5},{5,4},{6,7},{7,6},{8,9},{9,8},{10,11... | collective-permute-start | bytes 4718600 | tf_op jit(solution)/shard_map/ppermute | solution.py:99
